TPU v7x, 32 devices: a whole 2x2x4 slice. The times are simulated.
32 devices in a mesh: fs: 8 (over z, core), tp: 4 (over y, x).
Axes of the slice: x: 2, y: 2, z: 4, core: 2. Of those that a mesh axis runs over, the one named last changes fastest.
Arguments:
- tokens: bfloat16 [1024, 2048], P('fs'), may hold values from -6 to 6
- experts: int32 [1024, 4], P('fs'), may hold values from 0 to 7, all different within a row; in each aligned block of 128 rows (0 to 127, 128 to 255, ...) at most 96 rows name the same one
- routing: float32 [1024, 4], P('fs'), may hold values from 0.05 to 0.6
- norm_gain: float32 [2048], replicated, may hold values from 0.1 to 1.9
- gate_master: float32 [8, 2048, 2048], P(None, 'fs', 'tp'), may hold values from -0.625 to 0.625
- linear_master: float32 [8, 2048, 2048], P(None, 'fs', 'tp'), may hold values from -0.625 to 0.625
- down_weight: bfloat16 [8, 2048, 2048], P('fs', None, 'tp'), may hold values from -0.013671875 to 0.013671875
Outputs:
- gate_out: bfloat16 [8, 2048, 2048], P('fs', None, 'tp')
- linear_out: bfloat16 [8, 2048, 2048], P('fs', None, 'tp')
- expert_mix: bfloat16 [1024, 2048], P('fs', 'tp')
Inputs may be any that keep to these rules, and one draw needn't show every extreme that they name: Each row names 4 different experts; within the rows of one index of fs (aligned blocks of 128 rows) no expert is named by more than 96 rows, and in some blocks some expert is named by exactly 96; every expert is named somewhere.
All inputs are finite; a program needn't handle non-finite values.
Results may differ from a plain program's by a relative error of at most 0.023.
Values may be sent and summed in bfloat16 or wider, within the bound.
A program may use at most 64 MiB of HBM per device.

v0:
```python
import jax
import jax.numpy as jnp
from jax import lax
from jax.sharding import PartitionSpec as P

clamp_limit = 7.0
gate_slope = 1.702


def solution(mesh):
    n_fs, n_tp = (mesh.shape["fs"], mesh.shape["tp"])

    def on_device(tokens, experts, routing, norm_gain, gate_master, linear_master, down_weight):
        expert_count, depth, _ = gate_master.shape
        width = tokens.shape[1]
        fs, tp = (lax.axis_index("fs"), lax.axis_index("tp"))
        cols = width // n_tp
        mine = lax.dynamic_slice_in_dim(tokens, tp * cols, cols, axis=1)
        quarter = lax.all_gather(mine, "fs", axis=0, tiled=True)
        everyone = lax.all_gather(quarter, "tp", axis=1, tiled=True)
        choice = experts[:, :, None] == jnp.arange(expert_count, dtype=jnp.int32)[None, None, :]
        share = jnp.sum(jnp.where(choice, routing[:, :, None], 0.0), axis=1)
        shares = lax.all_gather(share, "fs", axis=0, tiled=True)
        share_mine = lax.dynamic_slice_in_dim(shares, fs, 1, axis=1)
        gain = lax.dynamic_slice_in_dim(norm_gain, fs * depth, depth, axis=0)[None, :, None]
        gate_out, linear_out = (
            lax.all_to_all(
                (master * gain).astype(jnp.bfloat16), "fs", split_axis=0, concat_axis=1, tiled=True
            )
            for master in (gate_master, linear_master)
        )
        pre_gate = jnp.dot(everyone, gate_out[0], preferred_element_type=jnp.float32)
        pre_linear = jnp.dot(everyone, linear_out[0], preferred_element_type=jnp.float32)
        clamped = jnp.minimum(pre_gate, clamp_limit)
        active = (
            clamped
            * jax.nn.sigmoid(gate_slope * clamped)
            * (jnp.clip(pre_linear, -clamp_limit, clamp_limit) + 1.0)
        ).astype(jnp.bfloat16)
        part = lax.dot_general(
            active, down_weight[0], (((1,), (1,)), ((), ())), preferred_element_type=jnp.float32
        )
        part = (part * share_mine).astype(jnp.bfloat16)
        summed = lax.psum_scatter(part, "tp", scatter_dimension=1, tiled=True)
        mixed = lax.psum_scatter(summed, "fs", scatter_dimension=0, tiled=True)
        return (gate_out, linear_out, mixed)

    placed = (
        P("fs", None),
        P("fs", None),
        P("fs", None),
        P(),
        P(None, "fs", "tp"),
        P(None, "fs", "tp"),
        P("fs", None, "tp"),
    )
    return jax.shard_map(
        on_device,
        mesh=mesh,
        in_specs=placed,
        out_specs=(P("fs", None, "tp"), P("fs", None, "tp"), P("fs", "tp")),
        check_vma=False,
    )
```

profile of v0, /device:TPU:0, one launch (start us, length us, event | category | flops | bytes accessed | tf_op | source)
XLA Modules:
  0.0 255.2 jit_solution(7410514343636466735)
XLA Ops:
  7.2 0.0 copy-start
  7.2 0.0 all-gather.3.cloned.1.call-start
  7.2 1.7 constant_dynamic-slice_fusion.1
  8.9 0.0 all-gather.3.cloned.1.call-update
  9.0 0.8 dynamic_slice.9
  9.7 6.8 %multiply_convert_fusion.1 = (bf16[8,256,512]{2,1,0:T(8,128)(2,1)}, bf16[8,256,512]{2,1,0:T(8,128)(2,1)}) fusion(f32[8,256,512]{2,1,0:T(8,128)} %param.12, f32[256]{0:T(256)S(1)} %dynamic_slice.9, f32[8,256,512]{2,1,0:T(8,128)} %param.11), kind=kLoop, calls=%fused_computation.1 | loop fusion | flops 4194304 | bytes 12583936 | tf_op jit(solution)/shard_map/convert_element_type | solution.py:28
  16.5 6.4 %all-to-all-start.1 = ((bf16[8,256,512]{2,1,0:T(8,128)(2,1)}), bf16[8,256,512]{2,1,0:T(8,128)(2,1)}, u32[]{:S(2)}, u32[]{:S(2)}) async-start(bf16[8,256,512]{2,1,0:T(8,128)(2,1)} %get-tuple-element.3), calls=%async_computation.1 | async-start | bytes 4194304 | tf_op jit(solution)/shard_map/all_to_all | solution.py:27
  22.9 0.0 all-gather.5.cloned.1.call-start
  22.9 17.5 %all-gather.3.cloned.1.call-done = bf16[1024,512]{1,0:T(8,128)(2,1)} async-done(((bf16[128,512]{1,0:T(8,128)(2,1)}), bf16[1024,512]{1,0:T(8,128)(2,1)}) %all-gather.3.cloned.1.call-update) | async-done | bytes 1048592 | tf_op jit(solution)/shard_map/all_gather | solution.py:19
  40.4 0.0 all-gather.5.cloned.1.call-update
  40.4 37.4 %all-to-all-done.1 = bf16[8,256,512]{2,1,0:T(8,128)(2,1)} async-done(((bf16[8,256,512]{2,1,0:T(8,128)(2,1)}), bf16[8,256,512]{2,1,0:T(8,128)(2,1)}, u32[]{:S(2)}, u32[]{:S(2)}) %all-to-all-start.1) | async-done | bytes 2097184 | tf_op jit(solution)/shard_map/all_to_all | solution.py:27
  77.8 0.0 copy-start.1
  77.8 0.0 copy-start.2
  77.8 4.5 %all-to-all-start = ((bf16[8,256,512]{2,1,0:T(8,128)(2,1)}), bf16[8,256,512]{2,1,0:T(8,128)(2,1)}, u32[]{:S(2)}, u32[]{:S(2)}) async-start(bf16[8,256,512]{2,1,0:T(8,128)(2,1)} %get-tuple-element.4), calls=%async_computation | async-start | bytes 4194304 | tf_op jit(solution)/shard_map/all_to_all | solution.py:27
  82.3 0.0 reduce-scatter.3.cloned.1.call-start
  82.4 0.0 copy-done.1
  82.4 0.0 copy-done.2
  82.4 55.0 %all_gather.11 = f32[1024,8]{0,1:T(8,128)S(1)} all-gather(f32[128,8]{0,1:T(8,128)S(1)} %select_reduce_fusion), channel_id=1, replica_groups=mesh['fs'=8,'tp'=4] {'fs'}, dimensions={0}, use_global_device_ids=true | all-gather | bytes 36864 | tf_op jit(solution)/shard_map/all_gather | solution.py:23
  137.4 0.0 all-gather.5.cloned.1.call-done
  137.5 6.5 %fusion.5 = f32[1024,512]{1,0:T(8,128)} fusion(bf16[1024,2048]{1,0:T(8,128)(2,1)} %all-gather.5.cloned.1.call-done, bf16[2048,512]{1,0:T(8,128)(2,1)} %bitcast.3), kind=kOutput, calls=%fused_computation.13 | convolution fusion | flops 2147483648 | bytes 8388608 | tf_op jit(solution)/shard_map/dot_general | solution.py:33
  144.0 0.0 all-to-all-done
  144.0 0.0 copy-done
  144.0 10.3 %multiply_convert_fusion = bf16[1024,2048]{1,0:T(8,128)(2,1)} fusion(f32[1024]{0:T(1024)S(1)} %bitcast.12, bf16[1,2048,512]{2,1,0:T(8,128)(2,1)S(1)} %copy-done, f32[1024,512]{1,0:T(8,128)} %fusion.5, bf16[1024,2048]{1,0:T(8,128)(2,1)} %all-gather.5.cloned.1.call-done, bf16[2048,512]{1,0:T(8,128)(2,1)} %bitcast.2), kind=kOutput, calls=%fused_computation | convolution fusion | flops 4304404480 | bytes 14684160 | tf_op jit(solution)/shard_map/dot_general | solution.py:40
  154.3 0.0 reduce-scatter.3.cloned.1.call-update
  154.3 0.0 reduce-scatter.5.cloned.1.call-start
  154.4 52.8 %reduce-scatter.3.cloned.1.call-done = bf16[1024,512]{1,0:T(8,128)(2,1)} async-done(((bf16[1024,2048]{1,0:T(8,128)(2,1)}), bf16[1024,512]{1,0:T(8,128)(2,1)}) %reduce-scatter.3.cloned.1.call-update) | async-done | bytes 1048592 | tf_op jit(solution)/shard_map/reduce_scatter | solution.py:44
  207.2 0.0 reduce-scatter.5.cloned.1.call-update
  207.2 35.4 %reduce-scatter.5.cloned.1.call-done = bf16[128,512]{1,0:T(8,128)(2,1)} async-done(((bf16[1024,512]{1,0:T(8,128)(2,1)}), bf16[128,512]{1,0:T(8,128)(2,1)}) %reduce-scatter.5.cloned.1.call-update) | async-done | bytes 131088 | tf_op jit(solution)/shard_map/reduce_scatter | solution.py:45
  242.6 3.0 %copy.16 = bf16[1,2048,512]{2,1,0:T(8,128)(2,1)} copy(bf16[1,2048,512]{2,1,0:T(8,128)(2,1)} %bitcast) | data formatting | bytes 4194304
  245.6 3.0 %copy.17 = bf16[1,2048,512]{2,1,0:T(8,128)(2,1)} copy(bf16[1,2048,512]{2,1,0:T(8,128)(2,1)} %bitcast.1) | data formatting | bytes 4194304
  (2 shorter events, 0.0 us)
Async XLA Ops:
  7.2 136.8 %copy-start = (bf16[1,2048,512]{2,1,0:T(8,128)(2,1)S(1)}, bf16[1,2048,512]{2,1,0:T(8,128)(2,1)}, u32[]{:S(2)}) copy-start(bf16[1,2048,512]{2,1,0:T(8,128)(2,1)} %param.13) | copy-start | bytes 6291460
  7.2 33.2 %all-gather.3.cloned.1.call-start = ((), (), s32[]{:S(2)}) async-start(), calls=%async_computation.4 | async-start | bytes 1179648 | tf_op jit(solution)/shard_map/all_gather | solution.py:19
  16.5 61.3 %all-to-all-start.1 = ((bf16[8,256,512]{2,1,0:T(8,128)(2,1)}), bf16[8,256,512]{2,1,0:T(8,128)(2,1)}, u32[]{:S(2)}, u32[]{:S(2)}) async-start(bf16[8,256,512]{2,1,0:T(8,128)(2,1)} %get-tuple-element.3), calls=%async_computation.1 | async-start | bytes 4194304 | tf_op jit(solution)/shard_map/all_to_all | solution.py:27
  22.9 114.6 %all-gather.5.cloned.1.call-start = ((), (), s32[]{:S(2)}) async-start(), calls=%async_computation.5 | async-start | bytes 5242880 | tf_op jit(solution)/shard_map/all_gather | solution.py:20
  77.8 4.6 %copy-start.1 = (f32[128,4]{0,1:T(4,128)S(1)}, f32[128,4]{0,1:T(4,128)}, u32[]{:S(2)}) copy-start(f32[128,4]{0,1:T(4,128)} %param.9) | copy-start | bytes 6148
  77.8 4.6 %copy-start.2 = (s32[128,4]{0,1:T(4,128)S(1)}, s32[128,4]{0,1:T(4,128)}, u32[]{:S(2)}) copy-start(s32[128,4]{0,1:T(4,128)} %param.8) | copy-start | bytes 6148
  77.8 66.2 %all-to-all-start = ((bf16[8,256,512]{2,1,0:T(8,128)(2,1)}), bf16[8,256,512]{2,1,0:T(8,128)(2,1)}, u32[]{:S(2)}, u32[]{:S(2)}) async-start(bf16[8,256,512]{2,1,0:T(8,128)(2,1)} %get-tuple-element.4), calls=%async_computation | async-start | bytes 4194304 | tf_op jit(solution)/shard_map/all_to_all | solution.py:27
  82.3 124.9 %reduce-scatter.3.cloned.1.call-start = ((), (), s32[]{:S(2)}) async-start(), calls=%async_computation.6 | async-start | bytes 5242880 | tf_op jit(solution)/shard_map/reduce_scatter | solution.py:44
  154.3 88.3 %reduce-scatter.5.cloned.1.call-start = ((), (), s32[]{:S(2)}) async-start(), calls=%async_computation.7 | async-start | bytes 1179648 | tf_op jit(solution)/shard_map/reduce_scatter | solution.py:45
Sparse Core Ops, SparseCore 0:
  10.2 30.2 all-gather.2
  42.2 56.2 all-gather.4
  154.4 52.7 reduce-scatter.2
  209.9 32.6 reduce-scatter.4
where the time goes:
time: 256 us; the launch traced here: 255 us
  waiting for transfers between devices  143 us (56%)
  blocking collectives  55 us (21%)
  matrix products  16.8 us (7%)
  between operations  13.8 us (5%)
  starting transfers between devices  11 us (4%)
  local copies, waits for them, and re-layouts  8.59 us (3%)
  other arithmetic  6.81 us (3%)
    all_gather x1, blocking collectives, on_device(): shares = lax.all_gather(share, 'fs', axis=0, tiled=True)  55 us
    reduce_scatter x1, waiting for transfers between devices, on_device(): summed = lax.psum_scatter(part, 'tp', scatter_dimension=1, tiled=True)  52.8 us
    all_to_all x2, waiting for transfers between devices, on_device(): lax.all_to_all((master * gain).astype(jnp.bfloat16), 'fs', split_axis=0,...  37.4 us
    reduce_scatter x1, waiting for transfers between devices, on_device(): mixed = lax.psum_scatter(summed, 'fs', scatter_dimension=0, tiled=True)  35.4 us
    all_gather x1, waiting for transfers between devices, on_device(): quarter = lax.all_gather(mine, 'fs', axis=0, tiled=True)  17.5 us
    all_to_all x2, starting transfers between devices, on_device(): lax.all_to_all((master * gain).astype(jnp.bfloat16), 'fs', split_axis=0,...  10.8 us
    dot_general x1, matrix products, on_device(): lax.dot_general(active, down_weight[0], (((1,), (1,)), ((), ())), preferr...  10.3 us
    convert_element_type x1, other arithmetic, on_device(): (master * gain).astype(jnp.bfloat16)  6.8 us
  transfers between devices with their start and end apart: 6, of which 4 were waited for; matrix products, arithmetic and copies ran while one was open for 6% of the time, Pallas kernels for 0%

commit v1 on v0

--- a/solution.py
+++ b/solution.py
@@ -17,7 +17,8 @@
         cols = width // n_tp
         mine = lax.dynamic_slice_in_dim(tokens, tp * cols, cols, axis=1)
         quarter = lax.all_gather(mine, "fs", axis=0, tiled=True)
-        everyone = lax.all_gather(quarter, "tp", axis=1, tiled=True)
+        repeated = jnp.stack([quarter] * lax.axis_size("tp"))
+        everyone = jnp.concatenate(lax.all_to_all(repeated, "tp", 0, 0), axis=1)
         choice = experts[:, :, None] == jnp.arange(expert_count, dtype=jnp.int32)[None, None, :]
         share = jnp.sum(jnp.where(choice, routing[:, :, None], 0.0), axis=1)
         shares = lax.all_gather(share, "fs", axis=0, tiled=True)

time: 256 us -> 307 us (1.20)
  blocking collectives: 55 us -> 106 us
    all_to_all x0 -> x1, blocking collectives: none -> 51.2 us  [on_device(): everyone = jnp.concatenate(lax.all_to_all(repeated, 'tp', 0, 0), axis=1)]
    all_to_all x2, waiting for transfers between devices: 37.4 us -> 22.1 us  [on_device(): lax.all_to_all((master * gain).astype(jnp.bfloat16), 'fs', split_axis=0,...]
    all_gather x1, waiting for transfers between devices: 17.5 us -> 32.3 us  [on_device(): quarter = lax.all_gather(mine, 'fs', axis=0, tiled=True)]
  transfers between devices with their start and end apart: 6 -> 5, of which waited for: 4 -> 4; matrix products, arithmetic and copies ran while one was open for 6% -> 3% of each run, Pallas kernels for 0% -> 0%
where the time goes in v1:
time: 307 us
  waiting for transfers between devices  141 us (46%)
  blocking collectives  106 us (35%)
  matrix products  16.9 us (6%)
  between operations  13.8 us (4%)
  starting transfers between devices  11 us (4%)
  local copies, waits for them, and re-layouts  10.6 us (3%)
  other arithmetic  6.81 us (2%)
    all_gather x1, blocking collectives, on_device(): shares = lax.all_gather(share, 'fs', axis=0, tiled=True)  55 us
    reduce_scatter x1, waiting for transfers between devices, on_device(): summed = lax.psum_scatter(part, 'tp', scatter_dimension=1, tiled=True)  51.4 us
    all_to_all x1, blocking collectives, on_device(): everyone = jnp.concatenate(lax.all_to_all(repeated, 'tp', 0, 0), axis=1)  51.2 us
    reduce_scatter x1, waiting for transfers between devices, on_device(): mixed = lax.psum_scatter(summed, 'fs', scatter_dimension=0, tiled=True)  35.4 us
    all_gather x1, waiting for transfers between devices, on_device(): quarter = lax.all_gather(mine, 'fs', axis=0, tiled=True)  32.3 us
    all_to_all x2, waiting for transfers between devices, on_device(): lax.all_to_all((master * gain).astype(jnp.bfloat16), 'fs', split_axis=0,...  22.1 us
    all_to_all x2, starting transfers between devices, on_device(): lax.all_to_all((master * gain).astype(jnp.bfloat16), 'fs', split_axis=0,...  10.8 us
    dot_general x1, matrix products, on_device(): lax.dot_general(active, down_weight[0], (((1,), (1,)), ((), ())), preferr...  10.3 us
  transfers between devices with their start and end apart: 5, of which 4 were waited for; matrix products, arithmetic and copies ran while one was open for 3% of the time, Pallas kernels for 0%

profile of v1, /device:TPU:0, one launch (start us, length us, event | category | flops | bytes accessed | tf_op | source)
XLA Modules:
  0.0 306.6 jit_solution(14991201083637401240)
XLA Ops:
  7.2 0.0 copy-start
  7.2 0.9 dynamic_slice.9
  8.1 6.8 %multiply_convert_fusion.1 = (bf16[8,256,512]{2,1,0:T(8,128)(2,1)}, bf16[8,256,512]{2,1,0:T(8,128)(2,1)}) fusion(f32[8,256,512]{2,1,0:T(8,128)} %param.12, f32[256]{0:T(256)S(1)} %dynamic_slice.9, f32[8,256,512]{2,1,0:T(8,128)} %param.11), kind=kLoop, calls=%fused_computation.1 | loop fusion | flops 4194304 | bytes 12583936 | tf_op jit(solution)/shard_map/convert_element_type | solution.py:29
  14.9 6.4 %all-to-all-start.1 = ((bf16[8,256,512]{2,1,0:T(8,128)(2,1)}), bf16[8,256,512]{2,1,0:T(8,128)(2,1)}, u32[]{:S(2)}, u32[]{:S(2)}) async-start(bf16[8,256,512]{2,1,0:T(8,128)(2,1)} %get-tuple-element.3), calls=%async_computation.1 | async-start | bytes 4194304 | tf_op jit(solution)/shard_map/all_to_all | solution.py:28
  21.3 0.0 all-gather.2.cloned.1.call-start
  21.3 1.6 constant_dynamic-slice_fusion.1
  22.9 0.0 all-gather.2.cloned.1.call-update
  22.9 32.3 %all-gather.2.cloned.1.call-done = bf16[1024,512]{1,0:T(8,128)(2,1)} async-done(((bf16[128,512]{1,0:T(8,128)(2,1)}), bf16[1024,512]{1,0:T(8,128)(2,1)}) %all-gather.2.cloned.1.call-update) | async-done | bytes 1048592 | tf_op jit(solution)/shard_map/all_gather | solution.py:19
  55.2 1.5 copy.15
  56.7 22.1 %all-to-all-done.1 = bf16[8,256,512]{2,1,0:T(8,128)(2,1)} async-done(((bf16[8,256,512]{2,1,0:T(8,128)(2,1)}), bf16[8,256,512]{2,1,0:T(8,128)(2,1)}, u32[]{:S(2)}, u32[]{:S(2)}) %all-to-all-start.1) | async-done | bytes 2097184 | tf_op jit(solution)/shard_map/all_to_all | solution.py:28
  78.8 0.5 stack.2
  79.3 51.2 %all_to_all.29 = bf16[4,1024,512]{1,2,0:T(8,128)(2,1)} all-to-all(bf16[4,1024,512]{1,2,0:T(8,128)(2,1)S(1)} %stack.2), channel_id=1, replica_groups=mesh['fs'=8,'tp'=4] {'tp'}, dimensions={0} | all-to-all | bytes 8388608 | tf_op jit(solution)/shard_map/all_to_all | solution.py:21
  130.6 0.0 copy-start.1
  130.6 0.0 copy-start.2
  130.6 4.5 %all-to-all-start = ((bf16[8,256,512]{2,1,0:T(8,128)(2,1)}), bf16[8,256,512]{2,1,0:T(8,128)(2,1)}, u32[]{:S(2)}, u32[]{:S(2)}) async-start(bf16[8,256,512]{2,1,0:T(8,128)(2,1)} %get-tuple-element.4), calls=%async_computation | async-start | bytes 4194304 | tf_op jit(solution)/shard_map/all_to_all | solution.py:28
  135.1 0.0 reduce-scatter.3.cloned.1.call-start
  135.1 0.0 copy-done.1
  135.1 0.0 copy-done.2
  135.2 55.0 %all_gather.7 = f32[1024,8]{0,1:T(8,128)S(1)} all-gather(f32[128,8]{0,1:T(8,128)S(1)} %select_reduce_fusion), channel_id=1, replica_groups=mesh['fs'=8,'tp'=4] {'fs'}, dimensions={0}, use_global_device_ids=true | all-gather | bytes 36864 | tf_op jit(solution)/shard_map/all_gather | solution.py:24
  190.2 6.6 %fusion.5 = f32[1024,512]{1,0:T(8,128)} fusion(bf16[1024,2048]{0,1:T(8,128)(2,1)} %bitcast.15, bf16[2048,512]{1,0:T(8,128)(2,1)} %bitcast.6), kind=kOutput, calls=%fused_computation.13 | convolution fusion | flops 2147483648 | bytes 8388608 | tf_op jit(solution)/shard_map/dot_general | solution.py:34
  196.8 0.0 all-to-all-done
  196.8 0.0 copy-done
  196.8 10.3 %multiply_convert_fusion = bf16[1024,2048]{1,0:T(8,128)(2,1)} fusion(f32[1024]{0:T(1024)S(1)} %bitcast.17, bf16[1,2048,512]{2,1,0:T(8,128)(2,1)S(1)} %copy-done, f32[1024,512]{1,0:T(8,128)} %fusion.5, bf16[1024,2048]{0,1:T(8,128)(2,1)} %bitcast.16, bf16[2048,512]{1,0:T(8,128)(2,1)} %bitcast.4), kind=kOutput, calls=%fused_computation | convolution fusion | flops 4304404480 | bytes 14684160 | tf_op jit(solution)/shard_map/dot_general | solution.py:41
  207.1 0.0 reduce-scatter.3.cloned.1.call-update
  207.1 0.0 reduce-scatter.5.cloned.1.call-start
  207.2 51.4 %reduce-scatter.3.cloned.1.call-done = bf16[1024,512]{1,0:T(8,128)(2,1)} async-done(((bf16[1024,2048]{1,0:T(8,128)(2,1)}), bf16[1024,512]{1,0:T(8,128)(2,1)}) %reduce-scatter.3.cloned.1.call-update) | async-done | bytes 1048592 | tf_op jit(solution)/shard_map/reduce_scatter | solution.py:45
  258.5 0.0 reduce-scatter.5.cloned.1.call-update
  258.6 35.4 %reduce-scatter.5.cloned.1.call-done = bf16[128,512]{1,0:T(8,128)(2,1)} async-done(((bf16[1024,512]{1,0:T(8,128)(2,1)}), bf16[128,512]{1,0:T(8,128)(2,1)}) %reduce-scatter.5.cloned.1.call-update) | async-done | bytes 131088 | tf_op jit(solution)/shard_map/reduce_scatter | solution.py:46
  294.0 3.0 copy.18
  297.0 3.0 copy.19
  (2 shorter events, 0.0 us)
Async XLA Ops:
  7.2 189.6 %copy-start = (bf16[1,2048,512]{2,1,0:T(8,128)(2,1)S(1)}, bf16[1,2048,512]{2,1,0:T(8,128)(2,1)}, u32[]{:S(2)}) copy-start(bf16[1,2048,512]{2,1,0:T(8,128)(2,1)} %param.13) | copy-start | bytes 6291460
  14.9 63.9 %all-to-all-start.1 = ((bf16[8,256,512]{2,1,0:T(8,128)(2,1)}), bf16[8,256,512]{2,1,0:T(8,128)(2,1)}, u32[]{:S(2)}, u32[]{:S(2)}) async-start(bf16[8,256,512]{2,1,0:T(8,128)(2,1)} %get-tuple-element.3), calls=%async_computation.1 | async-start | bytes 4194304 | tf_op jit(solution)/shard_map/all_to_all | solution.py:28
  21.3 34.0 %all-gather.2.cloned.1.call-start = ((), (), s32[]{:S(2)}) async-start(), calls=%async_computation.5 | async-start | bytes 1179648 | tf_op jit(solution)/shard_map/all_gather | solution.py:19
  130.6 4.6 %copy-start.1 = (f32[128,4]{0,1:T(4,128)S(1)}, f32[128,4]{0,1:T(4,128)}, u32[]{:S(2)}) copy-start(f32[128,4]{0,1:T(4,128)} %param.9) | copy-start | bytes 6148
  130.6 4.6 %copy-start.2 = (s32[128,4]{0,1:T(4,128)S(1)}, s32[128,4]{0,1:T(4,128)}, u32[]{:S(2)}) copy-start(s32[128,4]{0,1:T(4,128)} %param.8) | copy-start | bytes 6148
  130.6 66.2 %all-to-all-start = ((bf16[8,256,512]{2,1,0:T(8,128)(2,1)}), bf16[8,256,512]{2,1,0:T(8,128)(2,1)}, u32[]{:S(2)}, u32[]{:S(2)}) async-start(bf16[8,256,512]{2,1,0:T(8,128)(2,1)} %get-tuple-element.4), calls=%async_computation | async-start | bytes 4194304 | tf_op jit(solution)/shard_map/all_to_all | solution.py:28
  135.1 123.5 %reduce-scatter.3.cloned.1.call-start = ((), (), s32[]{:S(2)}) async-start(), calls=%async_computation.6 | async-start | bytes 5242880 | tf_op jit(solution)/shard_map/reduce_scatter | solution.py:45
  207.1 86.9 %reduce-scatter.5.cloned.1.call-start = ((), (), s32[]{:S(2)}) async-start(), calls=%async_computation.7 | async-start | bytes 1179648 | tf_op jit(solution)/shard_map/reduce_scatter | solution.py:46
Sparse Core Ops, SparseCore 0:
  24.2 30.9 all-gather.1
  207.2 51.2 reduce-scatter.2
  261.4 32.5 reduce-scatter.4
